TPU v7x, 32 devices: a whole 2x2x4 slice. The times are simulated.
32 devices in a mesh: grp: 2 (over y), fs: 4 (over z), tp: 4 (over x, core).
Axes of the slice: x: 2, y: 2, z: 4, core: 2. Of those that a mesh axis runs over, the one named last changes fastest.
Arguments:
- tokens: bfloat16 [2048, 4096], P(('grp', 'tp')), parts along dimension 0, may hold values from -6 to 6
- routes: int32 [2048, 2], P(('grp', 'tp')), parts along dimension 0, may hold values from 0 to 7, all different within a row; in each aligned block of 256 rows (0 to 255, 256 to 511, ...) at most 128 rows name the same one
- route_weight: float32 [2048, 2], P(('grp', 'tp')), parts along dimension 0, may hold values from 0.2 to 1
- norm_gain: float32 [4096], P('fs'), may hold values from 0.1 to 1.9
- gate_train: float32 [8, 4096, 2048], P(None, 'fs', 'tp'), may hold values from -0.09375 to 0.09375
- up_train: float32 [8, 4096, 2048], P(None, 'fs', 'tp'), may hold values from -0.09375 to 0.09375
- down_train: float32 [8, 2048, 4096], P(None, 'fs', 'tp'), may hold values from -0.125 to 0.125
Outputs:
- gate_serve: bfloat16 [16, 4096, 2048], P(('grp', 'tp'), None, 'fs'), parts along dimension 0
- up_serve: bfloat16 [16, 4096, 2048], P(('grp', 'tp'), None, 'fs'), parts along dimension 0
- down_serve: bfloat16 [16, 2048, 4096], P(('grp', 'tp'), 'fs'), parts along dimension 0
- moe_out: bfloat16 [2048, 4096], P(('grp', 'tp'), 'fs'), parts along dimension 0
There are 2 independent parts, one for each index of `grp`. A program takes and returns all parts, laid end to end along the dimension named above; an argument that names none is the same for every part. Nothing has to cross between parts.
Inputs may be any that keep to these rules, and one draw needn't show every extreme that they name: `routes`: within the 256 rows of each device (aligned blocks), no expert is named by more than 128 rows, a bound that some block reaches; the two experts of a row differ; every expert is named somewhere.
All inputs are finite; a program needn't handle non-finite values.
Results may differ from a plain program's by a relative error of at most 0.0076.
Values may be sent and summed in bfloat16 or wider, within the bound.
A program may use at most 192 MiB of HBM per device.

v0:
```python
import jax
import jax.numpy as jnp
from jax import lax
from jax.sharding import PartitionSpec as P

EXPERTS = 8
CAP = 128


def per_device(tokens, routes, route_weight, norm_gain, gate_train, up_train, down_train):
    gate_cast = (norm_gain[None, :, None] * gate_train).astype(jnp.bfloat16)
    up_cast = (norm_gain[None, :, None] * up_train).astype(jnp.bfloat16)
    down_cast = down_train.astype(jnp.bfloat16)
    gate_mid, up_mid, down_serve = (
        lax.all_to_all(gate_cast, "tp", split_axis=0, concat_axis=2, tiled=True),
        lax.all_to_all(up_cast, "tp", split_axis=0, concat_axis=2, tiled=True),
        lax.all_to_all(down_cast, "tp", split_axis=0, concat_axis=2, tiled=True),
    )
    gate_serve, up_serve = (
        lax.all_to_all(gate_mid, "fs", split_axis=2, concat_axis=1, tiled=True),
        lax.all_to_all(up_mid, "fs", split_axis=2, concat_axis=1, tiled=True),
    )
    tok_rows = tokens.shape[0]
    flat = routes.reshape(-1)
    expert_ids = jnp.arange(EXPERTS, dtype=jnp.int32)
    onehot = (flat[:, None] == expert_ids[None, :]).astype(jnp.int32)
    before = jnp.cumsum(onehot, axis=0) - onehot
    slot = jnp.sum(before * onehot, axis=1)
    place = (flat * CAP + slot).reshape(tok_rows, 2)
    slot_ids = jnp.arange(EXPERTS * CAP, dtype=jnp.int32)
    select = jnp.any(place[None, :, :] == slot_ids[:, None, None], axis=2).astype(jnp.bfloat16)
    outgoing = jnp.dot(select, tokens, preferred_element_type=jnp.float32).astype(jnp.bfloat16)
    arrived = lax.all_to_all(outgoing, "tp", split_axis=0, concat_axis=0, tiled=True)
    senders = lax.axis_size("tp")
    local = gate_serve.shape[0]
    arrived = arrived.reshape(senders, local, CAP, arrived.shape[1])
    gate_h = jnp.einsum("tlcd,ldf->tlcf", arrived, gate_serve, preferred_element_type=jnp.float32)
    up_h = jnp.einsum("tlcd,ldf->tlcf", arrived, up_serve, preferred_element_type=jnp.float32)
    hidden = (jax.nn.silu(gate_h) * up_h).astype(jnp.bfloat16)
    down_cols = lax.all_to_all(down_serve, "fs", split_axis=2, concat_axis=1, tiled=True)
    empty = jnp.zeros((down_cols.shape[2], senders * local * CAP), jnp.float32)
    term = jnp.einsum(
        "tlcf,lfd->dtlc",
        lax.all_gather(hidden, "fs", axis=3, tiled=True),
        down_cols,
        preferred_element_type=jnp.float32,
    )
    summed = term.reshape(empty.shape)
    returned = lax.all_to_all(
        summed.astype(jnp.bfloat16), "tp", split_axis=1, concat_axis=1, tiled=True
    )
    picked = jnp.take(returned, place, axis=1)
    mixed = (
        picked[:, :, 0].astype(jnp.float32) * route_weight[None, :, 0]
        + picked[:, :, 1].astype(jnp.float32) * route_weight[None, :, 1]
    )
    moe_out = mixed.T.astype(jnp.bfloat16)
    return (gate_serve, up_serve, down_serve, moe_out)


def solution(mesh):
    return jax.shard_map(
        per_device,
        mesh=mesh,
        in_specs=(
            P(("grp", "tp"), None),
            P(("grp", "tp"), None),
            P(("grp", "tp"), None),
            P("fs"),
            P(None, "fs", "tp"),
            P(None, "fs", "tp"),
            P(None, "fs", "tp"),
        ),
        out_specs=(
            P(("grp", "tp"), None, "fs"),
            P(("grp", "tp"), None, "fs"),
            P(("grp", "tp"), "fs", None),
            P(("grp", "tp"), "fs"),
        ),
        check_vma=False,
    )
```

profile of v0, /device:TPU:0, one launch (start us, length us, event | category | flops | bytes accessed | tf_op | source)
XLA Modules:
  0.0 1133.6 jit_solution(945579070629410904)
XLA Ops:
  23.4 17.0 %multiply_convert_fusion = (bf16[8,1024,512]{2,1,0:T(8,128)(2,1)}, bf16[8,1024,512]{2,1,0:T(8,128)(2,1)}) fusion(f32[8,1024,512]{2,1,0:T(8,128)} %param.12, f32[1024]{0:T(1024)S(1)} %copy-done.3, f32[8,1024,512]{2,1,0:T(8,128)} %param.11), kind=kLoop, calls=%fused_computation.1 | loop fusion | flops 16777216 | bytes 50335744 | tf_op jit(solution)/shard_map/convert_element_type | solution.py:12
  40.4 76.8 %all-to-all-done.5 = bf16[4,256,4096]{2,1,0:T(8,128)(2,1)} async-done(((bf16[4,256,4096]{2,1,0:T(8,128)(2,1)}), bf16[4,256,4096]{2,1,0:T(8,128)(2,1)}, u32[]{:S(2)}, u32[]{:S(2)}) %all-to-all-start.5) | async-done | bytes 8388640 | tf_op jit(solution)/shard_map/all_to_all | solution.py:33
  117.2 100.5 %all_to_all.126 = bf16[8,1024,512]{2,1,0:T(8,128)(2,1)} all-to-all(bf16[8,1024,512]{2,1,0:T(8,128)(2,1)} %get-tuple-element.30), channel_id=1, replica_groups=mesh['grp'=2,'fs'=4,'tp'=4] {'tp'}, dimensions={0} | all-to-all | bytes 16777216 | tf_op jit(solution)/shard_map/all_to_all | solution.py:16
  223.4 9.1 convert_element_type.53
  232.5 84.1 %all-to-all-done = bf16[8,1024,512]{2,1,0:T(8,128)(2,1)} async-done(((bf16[8,1024,512]{2,1,0:T(8,128)(2,1)}), bf16[8,1024,512]{2,1,0:T(8,128)(2,1)}, u32[]{:S(2)}, u32[]{:S(2)}) %all-to-all-start) | async-done | bytes 8388640 | tf_op jit(solution)/shard_map/all_to_all | solution.py:15
  322.1 11.4 %copy.99 = bf16[2,1024,4,512]{1,3,2,0:T(8,128)(2,1)} copy(bf16[2,1024,4,512]{3,1,0,2:T(8,128)(2,1)} %bitcast.96) | data formatting | bytes 16777216 | tf_op jit(solution)/shard_map/all_to_all | solution.py:16
  333.5 16.4 %copy.100 = bf16[2,1024,2048]{1,0,2:T(2,128)(2,1)} copy(bf16[2,1024,2048]{1,2,0:T(8,128)(2,1)} %bitcast.97) | data formatting | bytes 16777216 | tf_op jit(solution)/shard_map/all_to_all | solution.py:16
  349.9 65.4 %all-to-all-done.4 = bf16[8,512,1024]{2,1,0:T(8,128)(2,1)} async-done(((bf16[8,512,1024]{2,1,0:T(8,128)(2,1)}), bf16[8,512,1024]{2,1,0:T(8,128)(2,1)}, u32[]{:S(2)}, u32[]{:S(2)}) %all-to-all-start.4) | async-done | bytes 8388640 | tf_op jit(solution)/shard_map/all_to_all | solution.py:17
  421.0 11.4 %copy.95 = bf16[2,1024,4,512]{1,3,2,0:T(8,128)(2,1)} copy(bf16[2,1024,4,512]{3,1,0,2:T(8,128)(2,1)} %bitcast.1) | data formatting | bytes 16777216 | tf_op jit(solution)/shard_map/all_to_all | solution.py:15
  432.3 16.4 %copy.96 = bf16[2,1024,2048]{1,0,2:T(2,128)(2,1)} copy(bf16[2,1024,2048]{1,2,0:T(8,128)(2,1)} %bitcast.98) | data formatting | bytes 16777216 | tf_op jit(solution)/shard_map/all_to_all | solution.py:15
  448.7 156.0 %all-to-all-done.3 = bf16[2,1024,2048]{1,0,2:T(2,128)(2,1)} async-done(((bf16[2,1024,2048]{1,0,2:T(2,128)(2,1)}), bf16[2,1024,2048]{1,0,2:T(2,128)(2,1)}, u32[]{:S(2)}, u32[]{:S(2)}) %all-to-all-start.3) | async-done | bytes 8388640 | tf_op jit(solution)/shard_map/all_to_all | solution.py:21
  610.4 21.1 %copy.103 = bf16[4,2,512,1024]{2,1,3,0:T(2,128)(2,1)} copy(bf16[4,2,512,1024]{3,2,1,0:T(8,128)(2,1)} %bitcast.11) | data formatting | bytes 16777216 | tf_op jit(solution)/shard_map/all_to_all | solution.py:17
  631.5 161.5 %all-to-all-done.1 = bf16[2,1024,2048]{1,0,2:T(2,128)(2,1)} async-done(((bf16[2,1024,2048]{1,0,2:T(2,128)(2,1)}), bf16[2,1024,2048]{1,0,2:T(2,128)(2,1)}, u32[]{:S(2)}, u32[]{:S(2)}) %all-to-all-start.1) | async-done | bytes 8388640 | tf_op jit(solution)/shard_map/all_to_all | solution.py:20
  798.8 9.4 copy.101
  808.2 11.4 %copy.102 = bf16[2,4,1024,512]{3,2,1,0:T(8,128)(2,1)} copy(bf16[2,4,1024,512]{2,3,1,0:T(8,128)(2,1)} %bitcast.99) | data formatting | bytes 16777216 | tf_op jit(solution)/shard_map/all_to_all | solution.py:21
  819.6 9.3 copy.97
  828.9 12.2 %copy.98 = bf16[2,4,1024,512]{2,1,3,0:T(4,128)(2,1)} copy(bf16[2,4,1024,512]{2,3,1,0:T(8,128)(2,1)} %bitcast.93) | data formatting | bytes 16777216 | tf_op jit(solution)/shard_map/all_to_all | solution.py:20
  841.1 14.4 %reshape.71 = bf16[2,4096,512,1]{1,2,0,3:T(8,128)(2,1)} reshape(bf16[2,4,1024,512]{2,1,3,0:T(4,128)(2,1)} %copy.98) | data formatting | bytes 16777216 | tf_op jit(solution)/shard_map/all_to_all | solution.py:20
  855.5 10.3 fusion.2
  874.4 174.2 %all-to-all-done.6 = bf16[2,512,4096]{1,0,2:T(2,128)(2,1)} async-done(((bf16[2,512,4096]{1,0,2:T(2,128)(2,1)}), bf16[2,512,4096]{1,0,2:T(2,128)(2,1)}, u32[]{:S(2)}, u32[]{:S(2)}) %all-to-all-start.6) | async-done | bytes 8388640 | tf_op jit(solution)/shard_map/all_to_all | solution.py:40
  1048.6 21.0 %copy.110 = bf16[2,512,4,1024]{3,1,2,0:T(8,128)(2,1)} copy(bf16[2,512,4,1024]{1,0,3,2:T(2,128)(2,1)} %bitcast.23) | data formatting | bytes 16777216 | tf_op jit(solution)/shard_map/all_to_all | solution.py:40
  1069.6 9.2 convert_bitcast_fusion
  1085.7 21.0 %copy.116 = bf16[2,512,4096]{2,1,0:T(8,128)(2,1)} copy(bf16[2,512,4096]{1,0,2:T(2,128)(2,1)} %bitcast.92) | data formatting | bytes 16777216
  1106.7 11.4 %copy.123 = bf16[2,4,1024,512]{3,2,1,0:T(8,128)(2,1)} copy(bf16[2,4,1024,512]{2,3,1,0:T(8,128)(2,1)} %bitcast.94) | data formatting | bytes 16777216
  (52 shorter events, 68.6 us)
Async XLA Ops:
  7.2 4.7 copy-start
  17.6 5.8 copy-start.3
  17.6 99.6 %all-to-all-start.5 = ((bf16[4,256,4096]{2,1,0:T(8,128)(2,1)}), bf16[4,256,4096]{2,1,0:T(8,128)(2,1)}, u32[]{:S(2)}, u32[]{:S(2)}) async-start(bf16[4,256,4096]{2,1,0:T(8,128)(2,1)} %bitcast.95), calls=%async_computation.5 | async-start | bytes 16777216 | tf_op jit(solution)/shard_map/all_to_all | solution.py:33
  217.7 98.8 %all-to-all-start = ((bf16[8,1024,512]{2,1,0:T(8,128)(2,1)}), bf16[8,1024,512]{2,1,0:T(8,128)(2,1)}, u32[]{:S(2)}, u32[]{:S(2)}) async-start(bf16[8,1024,512]{2,1,0:T(8,128)(2,1)} %get-tuple-element.31), calls=%async_computation | async-start | bytes 16777216 | tf_op jit(solution)/shard_map/all_to_all | solution.py:15
  316.5 98.8 %all-to-all-start.4 = ((bf16[8,512,1024]{2,1,0:T(8,128)(2,1)}), bf16[8,512,1024]{2,1,0:T(8,128)(2,1)}, u32[]{:S(2)}, u32[]{:S(2)}) async-start(bf16[8,512,1024]{2,1,0:T(8,128)(2,1)} %convert_element_type.53), calls=%async_computation.4 | async-start | bytes 16777216 | tf_op jit(solution)/shard_map/all_to_all | solution.py:17
  415.3 189.4 %all-to-all-start.3 = ((bf16[2,1024,2048]{1,0,2:T(2,128)(2,1)}), bf16[2,1024,2048]{1,0,2:T(2,128)(2,1)}, u32[]{:S(2)}, u32[]{:S(2)}) async-start(bf16[2,1024,2048]{1,0,2:T(2,128)(2,1)} %copy.100), calls=%async_computation.3 | async-start | bytes 16777216 | tf_op jit(solution)/shard_map/all_to_all | solution.py:21
  604.7 188.2 %all-to-all-start.1 = ((bf16[2,1024,2048]{1,0,2:T(2,128)(2,1)}), bf16[2,1024,2048]{1,0,2:T(2,128)(2,1)}, u32[]{:S(2)}, u32[]{:S(2)}) async-start(bf16[2,1024,2048]{1,0,2:T(2,128)(2,1)} %copy.96), calls=%async_computation.1 | async-start | bytes 16777216 | tf_op jit(solution)/shard_map/all_to_all | solution.py:20
  792.9 255.7 %all-to-all-start.6 = ((bf16[2,512,4096]{1,0,2:T(2,128)(2,1)}), bf16[2,512,4096]{1,0,2:T(2,128)(2,1)}, u32[]{:S(2)}, u32[]{:S(2)}) async-start(bf16[2,512,4096]{1,0,2:T(2,128)(2,1)} %bitcast.91), calls=%async_computation.6 | async-start | bytes 16777216 | tf_op jit(solution)/shard_map/all_to_all | solution.py:40
  798.6 271.1 %all-gather.2.cloned.1.call-start = ((), (), s32[]{:S(2)}) async-start(), calls=%async_computation.8 | async-start | bytes 5242880 | tf_op jit(solution)/shard_map/all_gather | solution.py:44
  855.5 10.4 copy-start.2
  1078.8 6.3 copy-start.7
  1080.3 37.8 %all-to-all-start.7 = ((bf16[1024,4,256]{0,2,1:T(8,128)(2,1)}), bf16[1024,4,256]{0,2,1:T(8,128)(2,1)}, u32[]{:S(2)}, u32[]{:S(2)}) async-start(bf16[1024,4,256]{0,2,1:T(8,128)(2,1)} %bitcast.29), calls=%async_computation.7 | async-start | bytes 4194304 | tf_op jit(solution)/shard_map/all_to_all | solution.py:49
  1118.1 6.0 copy-start.4
  1118.1 7.6 copy-start.5
  1118.1 7.6 copy-start.6
  1118.1 8.7 copy-start.1
Sparse Core Ops, SparseCore 0:
  874.5 159.5 all-gather.1
where the time goes:
time: 1140 us; the launch traced here: 1130 us
  waiting for transfers between devices  718 us (63%)
  local copies, waits for them, and re-layouts  197 us (17%)
  blocking collectives  101 us (9%)
  starting transfers between devices  38.7 us (3%)
  matrix products  33.8 us (3%)
  other arithmetic  31.7 us (3%)
  between operations  14.3 us (1%)
    all_to_all x1, waiting for transfers between devices, per_device(): lax.all_to_all(down_serve, 'fs', split_axis=2, concat_axis=1, tiled=True)  174 us
    all_to_all x1, waiting for transfers between devices, per_device(): lax.all_to_all(gate_mid, 'fs', split_axis=2, concat_axis=1, tiled=True)  161 us
    all_to_all x1, waiting for transfers between devices, per_device(): lax.all_to_all(up_mid, 'fs', split_axis=2, concat_axis=1, tiled=True)  156 us
    all_to_all x1, blocking collectives, per_device(): lax.all_to_all(up_cast, 'tp', split_axis=0, concat_axis=2, tiled=True)  101 us
    all_to_all x1, waiting for transfers between devices, per_device(): lax.all_to_all(gate_cast, 'tp', split_axis=0, concat_axis=2, tiled=True)  84.1 us
    all_to_all x1, waiting for transfers between devices, per_device(): lax.all_to_all(outgoing, 'tp', split_axis=0, concat_axis=0, tiled=True)  76.8 us
    all_to_all x1, waiting for transfers between devices, per_device(): lax.all_to_all(down_cast, 'tp', split_axis=0, concat_axis=2, tiled=True)  65.4 us
    all_to_all x3, local copies, waits for them, and re-layouts, per_device(): lax.all_to_all(gate_mid, 'fs', split_axis=2, concat_axis=1, tiled=True)  35.8 us
  transfers between devices with their start and end apart: 8, of which 6 were waited for; matrix products, arithmetic and copies ran while one was open for 21% of the time, Pallas kernels for 0%

commit v1 on v0

v1 whole, which is shorter than its diff:
```python
import functools

import jax
import jax.numpy as jnp
from jax import lax
from jax.experimental import pallas as pl
from jax.experimental.pallas import tpu as pltpu
from jax.sharding import PartitionSpec as P

EXPERTS = 8
CAP = 128
MESH = pl.DeviceIdType.MESH


def interleaved(n):
    half = n // 2
    return [k // 2 + (k % 2) * half for k in range(n)]


def handoff(ngrp, nfs, ntp, gate, up, down, tok, gate_out, up_out, down_out, tok_out,
            stage, stage_sem, send_sem, recv_sem, dsend, drecv, tsend, trecv):
    g, f, t = lax.axis_index("grp"), lax.axis_index("fs"), lax.axis_index("tp")
    ratio = nfs // ntp
    local = gate_out.shape[0]
    rows = gate.shape[1]
    half = rows // 2
    width = gate_out.shape[2]
    other = 1 - g
    owner = f // ratio
    order = interleaved(ntp)

    barrier = pltpu.get_barrier_semaphore()

    def greet(dev, skip):
        @pl.when(jnp.logical_not(skip))
        def _():
            pl.semaphore_signal(barrier, inc=1, device_id=dev, device_id_type=MESH)

    for q in range(ratio):
        for k in range(ntp):
            greet((g, t * ratio + q, k), (f == t * ratio + q) & (t == k))
    for k in range(nfs):
        greet((g, k, owner), (f == k) & (t == owner))
    for k in range(1, ntp):
        greet((g, f, (t + k) % ntp), False)
    greet((other, f, t), False)
    total = ratio * ntp + nfs + ntp - 1 + 1
    me = (t == owner).astype(jnp.int32)
    pl.semaphore_wait(barrier, total - 2 * me)

    def chunk(src, out, dev_f, dev_t, q, l, h, m):
        e = dev_t * local + l
        return pltpu.make_async_remote_copy(
            src_ref=src.at[e, pl.ds(h * half, half), pl.ds(q * width, width)],
            dst_ref=out.at[l, pl.ds(f * rows + h * half, half), :],
            send_sem=send_sem.at[m, q, dev_t, l, h],
            recv_sem=recv_sem.at[m, l, f, h],
            device_id=(g, dev_f, dev_t), device_id_type=MESH)

    mats = ((gate, gate_out), (up, up_out))
    for m, (src, out) in enumerate(mats):
        for k in order:
            for l in range(local):
                for q in range(ratio):
                    dev_f, dev_t = t * ratio + q, (t + k) % ntp
                    for h in range(2):
                        send = (dev_f == f) | (g == h)
                        mine = (dev_f == f) & (dev_t == t)

                        @pl.when(send & jnp.logical_not(mine))
                        def _(src=src, out=out, q=q, l=l, h=h, m=m, dev_f=dev_f, dev_t=dev_t):
                            chunk(src, out, dev_f, dev_t, q, l, h, m).start()

    def tok_copy(k):
        n_tok = tok.shape[0]
        return pltpu.make_async_remote_copy(
            src_ref=tok, dst_ref=tok_out.at[pl.ds(t * n_tok, n_tok), :],
            send_sem=tsend.at[k - 1], recv_sem=trecv.at[k - 1],
            device_id=(g, f, (t + k) % ntp), device_id_type=MESH)

    for k in range(1, ntp):
        tok_copy(k).start()

    dcols = down.shape[2]

    def down_copy(k, l):
        return pltpu.make_async_remote_copy(
            src_ref=down.at[((t + k) % ntp) * local + l],
            dst_ref=down_out.at[l, :, pl.ds(t * dcols, dcols)],
            send_sem=dsend.at[k - 1, l], recv_sem=drecv.at[k - 1, l],
            device_id=(g, f, (t + k) % ntp), device_id_type=MESH)

    for k in range(1, ntp):
        for l in range(local):
            down_copy(k, l).start()

    def through(src, dst, buf, sem):
        load = pltpu.make_async_copy(src, buf, sem)
        load.start()
        load.wait()
        store = pltpu.make_async_copy(buf, dst, sem)
        store.start()
        store.wait()

    n_tok = tok.shape[0]
    through(tok, tok_out.at[pl.ds(t * n_tok, n_tok), :], stage[0], stage_sem)
    for l in range(local):
        through(down.at[t * local + l], down_out.at[l, :, pl.ds(t * dcols, dcols)],
                stage[1], stage_sem)

    @pl.when(t == owner)
    def _():
        q = f - t * ratio
        for m, (src, out) in enumerate(mats):
            for l in range(local):
                for qq in range(ratio):
                    @pl.when(q == qq)
                    def _(src=src, out=out, l=l, qq=qq):
                        through(src.at[t * local + l, :, pl.ds(qq * width, width)],
                                out.at[l, pl.ds(f * rows, rows), :], stage[2], stage_sem)

    def forward(m, out, l, fs_src):
        view = out.at[l, pl.ds(fs_src * rows + g * half, half), :]
        return pltpu.make_async_remote_copy(
            src_ref=view, dst_ref=view,
            send_sem=send_sem.at[m, ratio, fs_src % ntp, l, fs_src // ntp],
            recv_sem=recv_sem.at[m, l, fs_src, g],
            device_id=(other, f, t), device_id_type=MESH)

    def arrived(m, out, l, fs_src, h):
        view = out.at[l, pl.ds(fs_src * rows + h * half, half), :]
        pltpu.make_async_copy(view, view, recv_sem.at[m, l, fs_src, h]).wait()

    for m, (src, out) in enumerate(mats):
        for l in range(local):
            for d in range(1, nfs):
                fs_src = (f + d) % nfs
                arrived(m, out, l, fs_src, g)
                forward(m, out, l, fs_src).start()
    for m, (src, out) in enumerate(mats):
        for l in range(local):
            for d in range(1, nfs):
                arrived(m, out, l, (f + d) % nfs, other)

            @pl.when(t != owner)
            def _(m=m, out=out, l=l):
                for h in range(2):
                    arrived(m, out, l, f, h)
    for k in range(1, ntp):
        tok_copy(k).wait()
        for l in range(local):
            down_copy(k, l).wait()
    for m, (src, out) in enumerate(mats):
        for l in range(local):
            for d in range(1, nfs):
                forward(m, out, l, (f + d) % nfs).wait_send()
            for k in range(ntp):
                for q in range(ratio):
                    dev_f, dev_t = t * ratio + q, (t + k) % ntp
                    for h in range(2):
                        @pl.when(((dev_f == f) | (g == h)) & ((dev_f != f) | (dev_t != t)))
                        def _(src=src, out=out, q=q, l=l, h=h, m=m, dev_f=dev_f, dev_t=dev_t):
                            chunk(src, out, dev_f, dev_t, q, l, h, m).wait_send()


def move_weights(gate, up, down, tokens, nfs, ntp):
    local = EXPERTS // ntp
    width = gate.shape[2] * ntp // nfs
    rows, dcols = gate.shape[1], down.shape[2]
    dma = pltpu.SemaphoreType.DMA
    any_spec = pl.BlockSpec(memory_space=pl.ANY)
    bf = jnp.bfloat16
    ratio = nfs // ntp
    return pl.pallas_call(
        functools.partial(handoff, 2, nfs, ntp),
        out_shape=(
            jax.ShapeDtypeStruct((local, rows * nfs, width), bf),
            jax.ShapeDtypeStruct((local, rows * nfs, width), bf),
            jax.ShapeDtypeStruct((local, down.shape[1], dcols * ntp), bf),
            jax.ShapeDtypeStruct((tokens.shape[0] * ntp, tokens.shape[1]), bf),
        ),
        in_specs=[any_spec] * 4,
        out_specs=(any_spec,) * 4,
        scratch_shapes=[
            [pltpu.VMEM(tokens.shape, bf), pltpu.VMEM(down.shape[1:], bf),
             pltpu.VMEM((rows, width), bf)],
            dma,
            dma((2, ratio + 1, ntp, local, max(2, ratio))),
            dma((2, local, nfs, 2)),
            dma((ntp - 1, local)), dma((ntp - 1, local)),
            dma((ntp - 1,)), dma((ntp - 1,)),
        ],
        compiler_params=pltpu.CompilerParams(collective_id=0, has_side_effects=True),
    )(gate, up, down, tokens)


def per_device(tokens, routes, route_weight, norm_gain, gate_train, up_train, down_train):
    nfs, ntp = lax.axis_size("fs"), lax.axis_size("tp")
    t = lax.axis_index("tp")
    bf = jnp.bfloat16
    gate_cast = (norm_gain[None, :, None] * gate_train).astype(bf)
    up_cast = (norm_gain[None, :, None] * up_train).astype(bf)
    down_cast = down_train.astype(bf)
    gate_serve, up_serve, down_serve, tok_all = move_weights(
        gate_cast, up_cast, down_cast, tokens, nfs, ntp)
    local = EXPERTS // ntp
    n_tok = tokens.shape[0]
    routes_all = lax.all_gather(routes, "tp", axis=0)
    weight_all = lax.all_gather(route_weight, "tp", axis=0)
    expert_ids = jnp.arange(EXPERTS, dtype=jnp.int32)
    named = routes_all[None] == expert_ids[:, None, None, None]
    chosen = jnp.any(named, axis=3)
    weight_e = jnp.sum(jnp.where(named, weight_all[None], 0.0), axis=3)
    count = chosen.astype(jnp.int32)
    slot = jnp.cumsum(count, axis=2) - count
    slot_ids = jnp.arange(CAP, dtype=jnp.int32)
    select = (chosen[:, :, None, :] & (slot[:, :, None, :] == slot_ids[None, None, :, None])).astype(bf)
    mine = lax.dynamic_slice_in_dim(select, t * local, local, axis=0)
    weight_mine = lax.dynamic_slice_in_dim(weight_e, t * local, local, axis=0)
    gate_h = jnp.einsum("td,ldf->ltf", tok_all, gate_serve, preferred_element_type=jnp.float32)
    up_h = jnp.einsum("td,ldf->ltf", tok_all, up_serve, preferred_element_type=jnp.float32)
    hidden = jax.nn.silu(gate_h) * up_h * weight_mine.reshape(local, -1)[:, :, None]
    hidden = hidden.astype(bf).reshape(local, ntp, n_tok, -1)
    packed = jnp.einsum("lbst,lbtf->lbsf", mine, hidden, preferred_element_type=jnp.float32).astype(bf)
    packed = lax.all_gather(packed, "tp", axis=0, tiled=True)
    dense = jnp.einsum("ebst,ebsf->btef", select, packed, preferred_element_type=jnp.float32).astype(bf)
    partial = jnp.dot(
        dense.reshape(ntp * n_tok, -1), down_cast.reshape(-1, down_cast.shape[2]),
        preferred_element_type=jnp.float32).astype(bf)
    ratio = nfs // ntp
    partial = partial.reshape(ntp, n_tok, ratio, -1)
    partial = lax.all_to_all(partial, "tp", split_axis=0, concat_axis=0, tiled=True)
    partial = partial.transpose(0, 2, 1, 3).reshape(nfs, n_tok, -1)
    partial = lax.all_to_all(partial, "fs", split_axis=0, concat_axis=0, tiled=True)
    moe_out = jnp.sum(partial.astype(jnp.float32), axis=0).astype(bf)
    return (gate_serve, up_serve, down_serve, moe_out)


def solution(mesh):
    return jax.shard_map(
        per_device,
        mesh=mesh,
        in_specs=(
            P(("grp", "tp"), None),
            P(("grp", "tp"), None),
            P(("grp", "tp"), None),
            P("fs"),
            P(None, "fs", "tp"),
            P(None, "fs", "tp"),
            P(None, "fs", "tp"),
        ),
        out_specs=(
            P(("grp", "tp"), None, "fs"),
            P(("grp", "tp"), None, "fs"),
            P(("grp", "tp"), "fs", None),
            P(("grp", "tp"), "fs"),
        ),
        check_vma=False,
    )
```

time: 1140 us -> 686 us (0.60)
  waiting for transfers between devices: 718 us -> 81.3 us
  Pallas kernels: 0 us -> 410 us
  local copies, waits for them, and re-layouts: 197 us -> 49.7 us
  blocking collectives: 101 us -> 40.6 us
  starting transfers between devices: 38.7 us -> 4.63 us
  matrix products: 33.8 us -> 53.8 us
    all_to_all x7 -> x1, waiting for transfers between devices: 718 us -> 47.8 us  [per_device(): lax.all_to_all(partial, 'fs', split_axis=0, concat_axis=0, tiled=True)]
    pallas_call x0 -> x1, Pallas kernels: none -> 410 us  [move_weights(): pl.pallas_call(functools.partial(handoff, 2, nfs, ntp), out_shape=(jax.Sh...]
    all_to_all x11 -> x0, local copies, waits for them, and re-layouts: 154 us -> none  [the longest x3 35.8 us: per_device(): lax.all_to_all(gate_mid, 'fs', split_axis=2, concat_axis=1, tiled=True)]
    all_to_all x1, blocking collectives: 101 us -> 29 us  [per_device(): lax.all_to_all(partial, 'tp', split_axis=0, concat_axis=0, tiled=True)]
    all_to_all x7 -> x1, starting transfers between devices: 38.5 us -> 4.6 us  [per_device(): lax.all_to_all(partial, 'fs', split_axis=0, concat_axis=0, tiled=True)]
    all_gather x1, waiting for transfers between devices: 0.01 us -> 33.5 us  [per_device(): packed = lax.all_gather(packed, 'tp', axis=0, tiled=True)]
    dot_general x4 -> x5, matrix products: 33.8 us -> 53.8 us  [the longest x1 15.2 us: per_device(): jnp.einsum('td,ldf->ltf', tok_all, gate_serve, preferred_element_type=jnp...]
    convert_element_type x1, local copies, waits for them, and re-layouts: 1.48 us -> 14.5 us  [per_device(): jnp.einsum('ebst,ebsf->btef', select, packed, preferred_element_type=jnp....]
  transfers between devices with their start and end apart: 8 -> 2, of which waited for: 6 -> 2; matrix products, arithmetic and copies ran while one was open for 21% -> 0% of each run, Pallas kernels for 0% -> 0%
where the time goes in v1:
time: 686 us; the launch traced here: 685 us
  Pallas kernels  410 us (60%)
  waiting for transfers between devices  81.3 us (12%)
  matrix products  53.8 us (8%)
  local copies, waits for them, and re-layouts  49.7 us (7%)
  blocking collectives  40.6 us (6%)
  other arithmetic  30.7 us (4%)
  between operations  14.1 us (2%)
    pallas_call x1, Pallas kernels, move_weights(): pl.pallas_call(functools.partial(handoff, 2, nfs, ntp), out_shape=(jax.Sh...  410 us
    all_to_all x1, waiting for transfers between devices, per_device(): lax.all_to_all(partial, 'fs', split_axis=0, concat_axis=0, tiled=True)  47.8 us
    unnamed x10, local copies, waits for them, and re-layouts  34.9 us
    all_gather x1, waiting for transfers between devices, per_device(): packed = lax.all_gather(packed, 'tp', axis=0, tiled=True)  33.5 us
    all_to_all x1, blocking collectives, per_device(): lax.all_to_all(partial, 'tp', split_axis=0, concat_axis=0, tiled=True)  29 us
    convert_element_type x1, other arithmetic, per_device(): up_cast = (norm_gain[None, :, None] * up_train).astype(bf)  17 us
    dot_general x1, matrix products, per_device(): jnp.einsum('td,ldf->ltf', tok_all, gate_serve, preferred_element_type=jnp...  15.2 us
    dot_general x1, matrix products, per_device(): jnp.einsum('td,ldf->ltf', tok_all, up_serve, preferred_element_type=jnp.f...  15.1 us
  transfers between devices with their start and end apart: 2, of which 2 were waited for; matrix products, arithmetic and copies ran while one was open for 0% of the time, Pallas kernels for 0%

profile of v1, /device:TPU:0, one launch (start us, length us, event | category | flops | bytes accessed | tf_op | source)
XLA Modules:
  0.0 685.1 jit_solution(2677444838983761649)
XLA Ops:
  7.2 9.1 %convert_element_type.42.down = bf16[8,512,1024]{2,1,0:T(8,128)(2,1)} convert(f32[8,512,1024]{2,1,0:T(8,128)} %param.13) | non-fusion elementwise | flops 4194304 | bytes 25165824 | tf_op jit(solution)/shard_map/convert_element_type | solution.py:203
  16.3 6.2 all-gather
  22.5 5.5 all-gather.1
  28.0 2.3 reduce-window.6
  30.3 0.3 slice_reduce_fusion
  30.6 0.1 convert_subtract_fusion
  30.7 0.9 fusion.9
  31.6 17.0 %multiply_convert_fusion = (bf16[8,1024,512]{2,1,0:T(8,128)(2,1)}, bf16[8,1024,512]{2,1,0:T(8,128)(2,1)}) fusion(f32[8,1024,512]{2,1,0:T(8,128)} %param.12, f32[1024]{0:T(1024)S(1)} %copy-done, f32[8,1024,512]{2,1,0:T(8,128)} %param.11), kind=kLoop, calls=%fused_computation | loop fusion | flops 16777216 | bytes 50335744 | tf_op jit(solution)/shard_map/convert_element_type | solution.py:202
  48.6 410.2 %shard_map.102 = (bf16[2,4096,512]{2,1,0:T(8,128)(2,1)}, bf16[2,4096,512]{2,1,0:T(8,128)(2,1)}, bf16[2,512,4096]{2,1,0:T(8,128)(2,1)}, bf16[1024,4096]{1,0:T(8,128)(2,1)}) custom-call(bf16[8,1024,512]{2,1,0:T(8,128)(2,1)} %get-tuple-element.13.gate, bf16[8,1024,512]{2,1,0:T(8,128)(2,1)} %get-tuple-element.12.up, ...), custom_call_target="tpu_custom_call" | custom-call | tf_op jit(solution)/shard_map/pallas_call | solution.py:174
  458.8 15.1 %fusion = f32[2,512,1024]{2,1,0:T(8,128)} fusion(bf16[2,4096,512]{2,1,0:T(8,128)(2,1)} %get-tuple-element.19, bf16[1024,4096]{1,0:T(8,128)(2,1)} %get-tuple-element.11), kind=kOutput, calls=%fused_computation.2 | convolution fusion | flops 8589934592 | bytes 20971520 | tf_op jit(solution)/shard_map/td,ldf->ltf/dot_general | solution.py:221
  473.9 15.2 %fusion.5 = bf16[2,1024,512]{1,2,0:T(8,128)(2,1)S(1)} fusion(f32[2,512,1024]{2,1,0:T(8,128)} %fusion, bf16[2,4096,512]{2,1,0:T(8,128)(2,1)} %get-tuple-element.18, bf16[1024,4096]{1,0:T(8,128)(2,1)} %get-tuple-element.11, f32[2,1024]{1,0:T(2,128)S(1)} %bitcast.70), kind=kOutput, calls=%fused_computation.9 | convolution fusion | flops 8597274624 | bytes 23076864 | tf_op jit(solution)/shard_map/td,ldf->ltf/dot_general | solution.py:220
  489.2 1.8 fusion.15
  491.0 33.5 %all-gather.4.cloned.1.call-done = bf16[8,4,128,512]{3,2,0,1:T(8,128)(2,1)} async-done(((bf16[2,4,128,512]{3,2,0,1:T(8,128)(2,1)}), bf16[8,4,128,512]{3,2,0,1:T(8,128)(2,1)}) %all-gather.4.cloned.1.call-update) | async-done | bytes 4194320 | tf_op jit(solution)/shard_map/all_gather | solution.py:225
  524.5 8.0 %convert_bitcast_fusion = bf16[4,256,8,512]{1,3,2,0:T(8,128)(2,1)} fusion(bf16[8,4,128,512]{3,2,0,1:T(8,128)(2,1)} %all-gather.4.cloned.1.call-done, s32[8,4,256]{2,0,1:T(8,128)S(1)} %convert_subtract_fusion, pred[8,4,256]{2,0,1:T(8,128)(4,1)S(1)} %fusion.19), kind=kOutput, calls=%fused_computation.6 | convolution fusion | flops 1080033280 | bytes 12623872 | tf_op jit(solution)/shard_map/ebst,ebsf->btef/dot_general | solution.py:226
  532.5 14.5 %copy.40 = bf16[4,256,8,512]{3,2,1,0:T(8,128)(2,1)} copy(bf16[4,256,8,512]{1,3,2,0:T(8,128)(2,1)} %convert_bitcast_fusion) | data formatting | bytes 16777216 | tf_op jit(solution)/shard_map/convert_element_type | solution.py:226
  547.0 12.4 %copy.48 = bf16[128,8,8,512]{3,1,2,0:T(8,128)(2,1)} copy(bf16[128,8,8,512]{3,2,1,0:T(8,128)(2,1)} %bitcast.62) | data formatting | bytes 16777216
  559.4 13.7 %convolution_convert_fusion = bf16[1024,1024]{1,0:T(8,128)(2,1)S(1)} fusion(bf16[1024,4096]{1,0:T(8,128)(2,1)} %bitcast.63, bf16[4096,1024]{1,0:T(8,128)(2,1)} %bitcast.61), kind=kOutput, calls=%fused_computation.20 | convolution fusion | flops 8590983168 | bytes 18874368 | tf_op jit(solution)/shard_map/dot_general | solution.py:227
  573.0 29.0 %all_to_all.10 = bf16[4,256,1,1024]{3,1,2,0:T(8,128)(2,1)} all-to-all(bf16[4,256,1,1024]{3,1,2,0:T(8,128)(2,1)S(1)} %bitcast.66), channel_id=1, replica_groups=mesh['grp'=2,'fs'=4,'tp'=4] {'tp'}, dimensions={0} | all-to-all | bytes 4194304 | tf_op jit(solution)/shard_map/all_to_all | solution.py:232
  602.0 4.6 all-to-all-start.1
  606.6 47.8 %all-to-all-done.1 = bf16[4,256,1024]{2,1,0:T(8,128)(2,1)S(1)} async-done(((bf16[4,256,1024]{2,1,0:T(8,128)(2,1)}), bf16[4,256,1024]{2,1,0:T(8,128)(2,1)S(1)}, u32[]{:S(2)}, u32[]{:S(2)}) %all-to-all-start.1) | async-done | bytes 2097184 | tf_op jit(solution)/shard_map/all_to_all | solution.py:234
  654.4 1.3 reduce_sum.22
  655.7 7.3 %copy.62 = bf16[2,4096,512]{2,1,0:T(8,128)(2,1)} copy(bf16[2,4096,512]{2,1,0:T(8,128)(2,1)} %get-tuple-element.18) | data formatting | bytes 16777216
  663.0 7.3 %copy.63 = bf16[2,4096,512]{2,1,0:T(8,128)(2,1)} copy(bf16[2,4096,512]{2,1,0:T(8,128)(2,1)} %get-tuple-element.19) | data formatting | bytes 16777216
  670.3 7.9 %copy.64 = bf16[2,512,4096]{2,1,0:T(8,128)(2,1)} copy(bf16[2,512,4096]{2,1,0:T(8,128)(2,1)} %get-tuple-element.20) | data formatting | bytes 16777216
  (14 shorter events, 0.1 us)
Async XLA Ops:
  7.2 517.3 %all-gather.4.cloned.1.call-start = ((), (), s32[]{:S(2)}) async-start(), calls=%async_computation.2 | async-start | bytes 5242880 | tf_op jit(solution)/shard_map/all_gather | solution.py:225
  7.2 9.1 %copy-start.1 = (s32[256,2]{0,1:T(2,128)S(1)}, s32[256,2]{0,1:T(2,128)}, u32[]{:S(2)}) copy-start(s32[256,2]{0,1:T(2,128)} %param.8) | copy-start | bytes 6148
  7.2 15.3 %copy-start.2 = (f32[256,2]{0,1:T(2,128)S(1)}, f32[256,2]{0,1:T(2,128)}, u32[]{:S(2)}) copy-start(f32[256,2]{0,1:T(2,128)} %param.9) | copy-start | bytes 6148
  7.2 24.4 %copy-start = (f32[1024]{0:T(1024)S(1)}, f32[1024]{0:T(1024)}, u32[]{:S(2)}) copy-start(f32[1024]{0:T(1024)} %param.10) | copy-start | bytes 12292
  602.0 52.4 %all-to-all-start.1 = ((bf16[4,256,1024]{2,1,0:T(8,128)(2,1)}), bf16[4,256,1024]{2,1,0:T(8,128)(2,1)S(1)}, u32[]{:S(2)}, u32[]{:S(2)}) async-start(bf16[4,256,1024]{2,1,0:T(8,128)(2,1)} %bitcast.64), calls=%async_computation.1 | async-start | bytes 4194304 | tf_op jit(solution)/shard_map/all_to_all | solution.py:234
Sparse Core Ops, SparseCore 0:
  491.1 33.3 all-gather.3

commit v2 on v1

v2 whole, which is shorter than its diff:
```python
import functools

import jax
import jax.numpy as jnp
from jax import lax
from jax.experimental import pallas as pl
from jax.experimental.pallas import tpu as pltpu
from jax.sharding import PartitionSpec as P

EXPERTS = 8
CAP = 128
MESH = pl.DeviceIdType.MESH


def handoff(nfs, ntp, gate, up, down, tok, gate_out, up_out, down_out, tok_out, relay,
            stage, stage_sem, send_sem, recv_sem, hand_sem, pass_send, pass_recv,
            dsend, drecv, tsend, trecv):
    g, f, t = lax.axis_index("grp"), lax.axis_index("fs"), lax.axis_index("tp")
    ratio = nfs // ntp
    chips = ntp // 2
    local = gate_out.shape[0]
    rows = gate.shape[1]
    half = rows // 2
    width = gate_out.shape[2]
    other = 1 - g
    owner = f // ratio
    base = (t // 2) * 2
    mate = base + 1 - t % 2

    barrier = pltpu.get_barrier_semaphore()

    def greet(dev, skip):
        @pl.when(jnp.logical_not(skip))
        def _():
            pl.semaphore_signal(barrier, inc=1, device_id=dev, device_id_type=MESH)

    for j in range(chips):
        for q in range(ratio):
            for tc in range(2):
                dev_f = ((t + ntp - 2 * j) % ntp) * ratio + q
                greet((g, dev_f, base + tc), (f == dev_f) & (t == base + tc))
    for k in range(nfs):
        greet((g, k, base + owner % 2), (f == k) & (t % 2 == owner % 2))
    for k in range(1, ntp):
        greet((g, f, (t + k) % ntp), False)
    greet((other, f, t), False)
    me = (t % 2 == owner % 2).astype(jnp.int32)
    pl.semaphore_wait(barrier, 2 * nfs - 2 * me + ntp)

    mats = ((gate, gate_out), (up, up_out))
    steps = [(m, l) for m in range(2) for l in range(local)]

    def chunk(m, l, j, tc, q, h):
        src, out = mats[m]
        dev_t = ((t + 2 * j) % ntp) // 2 * 2 + tc
        return pltpu.make_async_remote_copy(
            src_ref=src.at[dev_t * local + l, pl.ds(h * half, half), pl.ds(q * width, width)],
            dst_ref=out.at[l, pl.ds(f * rows + h * half, half), :],
            send_sem=send_sem.at[m, l, j, tc, q, h],
            recv_sem=recv_sem.at[m, l, f, h],
            device_id=(g, t * ratio + q, dev_t), device_id_type=MESH)

    def hop(m, l, j, tc, q):
        src, _ = mats[m]
        near = (t + 2 * j) % ntp
        return pltpu.make_async_remote_copy(
            src_ref=src.at[(near // 2 * 2 + tc) * local + l, pl.ds(g * half, half),
                           pl.ds(q * width, width)],
            dst_ref=relay.at[m, l, j - 1, tc, q],
            send_sem=send_sem.at[m, l, j, tc, q, 0],
            recv_sem=pass_recv.at[m, l, j - 1, tc, q],
            device_id=(g, f, near), device_id_type=MESH)

    def onward(m, l, j, tc, q):
        _, out = mats[m]
        came = (t + ntp - 2 * j) % ntp
        return pltpu.make_async_remote_copy(
            src_ref=relay.at[m, l, j - 1, tc, q],
            dst_ref=out.at[l, pl.ds(f * rows + g * half, half), :],
            send_sem=pass_send.at[m, l, j - 1, tc, q],
            recv_sem=recv_sem.at[m, l, f, g],
            device_id=(g, came * ratio + q, base + tc), device_id_type=MESH)

    def each_send(act):
        for m, l in steps:
            for tc in range(2):
                for j in range(chips):
                    for q in range(ratio):
                        far = t * ratio + q != f
                        if j == 0:
                            for h in range(2):
                                @pl.when((far & (g == h)) | (jnp.logical_not(far) & (base + tc != t)))
                                def _(h=h):
                                    act(chunk(m, l, j, tc, q, h))
                        else:
                            @pl.when(far)
                            def _():
                                act(hop(m, l, j, tc, q))

                            @pl.when(jnp.logical_not(far))
                            def _():
                                for h in range(2):
                                    act(chunk(m, l, j, tc, q, h))

    each_send(lambda copy: copy.start())

    n_tok = tok.shape[0]

    def tok_copy(j):
        return pltpu.make_async_remote_copy(
            src_ref=tok, dst_ref=tok_out.at[pl.ds(t * n_tok, n_tok), :],
            send_sem=tsend.at[0, j], recv_sem=trecv.at[t],
            device_id=(g, f, (t + 2 * j) % ntp if j else mate), device_id_type=MESH)

    def tok_view(who):
        return tok_out.at[pl.ds(who * n_tok, n_tok), :]

    def tok_share(j):
        came = (t + ntp - 2 * j) % ntp
        return pltpu.make_async_remote_copy(
            src_ref=tok_view(came), dst_ref=tok_view(came),
            send_sem=tsend.at[1, j], recv_sem=trecv.at[came],
            device_id=(g, f, mate), device_id_type=MESH)

    def tok_arrived(who):
        pltpu.make_async_copy(tok_view(who), tok_view(who), trecv.at[who]).wait()

    for j in range(chips):
        tok_copy(j).start()

    dcols = down.shape[2]

    def down_copy(k, l):
        return pltpu.make_async_remote_copy(
            src_ref=down.at[((t + k) % ntp) * local + l],
            dst_ref=down_out.at[l, :, pl.ds(t * dcols, dcols)],
            send_sem=dsend.at[k - 1, l], recv_sem=drecv.at[k - 1, l],
            device_id=(g, f, (t + k) % ntp), device_id_type=MESH)

    for k in range(1, ntp):
        for l in range(local):
            down_copy(k, l).start()

    def through(src, dst, buf, sem):
        load = pltpu.make_async_copy(src, buf, sem)
        load.start()
        load.wait()
        store = pltpu.make_async_copy(buf, dst, sem)
        store.start()
        store.wait()

    through(tok, tok_view(t), stage[0], stage_sem)
    for l in range(local):
        through(down.at[t * local + l], down_out.at[l, :, pl.ds(t * dcols, dcols)],
                stage[1], stage_sem)

    @pl.when(t == owner)
    def _():
        for m, (src, out) in enumerate(mats):
            for l in range(local):
                for q in range(ratio):
                    @pl.when(f - t * ratio == q)
                    def _():
                        through(src.at[t * local + l, :, pl.ds(q * width, width)],
                                out.at[l, pl.ds(f * rows, rows), :], stage[2], stage_sem)

    def relayed(act):
        def step(m, l):
            for tc in range(2):
                for j in range(1, chips):
                    for q in range(ratio):
                        came = (t + ntp - 2 * j) % ntp

                        @pl.when(came * ratio + q != f)
                        def _():
                            act(m, l, j, tc, q)
        return step

    def pass_on(m, l, j, tc, q):
        view = relay.at[m, l, j - 1, tc, q]
        pltpu.make_async_copy(view, view, pass_recv.at[m, l, j - 1, tc, q]).wait()
        onward(m, l, j, tc, q).start()

    def forward(m, l, fs_src):
        view = mats[m][1].at[l, pl.ds(fs_src * rows + g * half, half), :]
        return pltpu.make_async_remote_copy(
            src_ref=view, dst_ref=view,
            send_sem=hand_sem.at[m, l, fs_src],
            recv_sem=recv_sem.at[m, l, fs_src, g],
            device_id=(other, f, t), device_id_type=MESH)

    def arrived(m, l, fs_src, h):
        view = mats[m][1].at[l, pl.ds(fs_src * rows + h * half, half), :]
        pltpu.make_async_copy(view, view, recv_sem.at[m, l, fs_src, h]).wait()

    def hand_on(m, l):
        for d in range(1, nfs):
            fs_src = (f + d) % nfs
            arrived(m, l, fs_src, g)
            forward(m, l, fs_src).start()

    ahead = relayed(pass_on)
    ahead(*steps[0])
    for i, step in enumerate(steps):
        if i + 1 < len(steps):
            ahead(*steps[i + 1])
        if i + 1 == len(steps):
            for j in range(1, chips):
                tok_arrived((t + ntp - 2 * j) % ntp)
                tok_share(j).start()
        hand_on(*step)

    for m, l in steps:
        for d in range(1, nfs):
            arrived(m, l, (f + d) % nfs, other)

        @pl.when(t != owner)
        def _():
            for h in range(2):
                arrived(m, l, f, h)
    tok_arrived(mate)
    for j in range(1, chips):
        tok_arrived((mate + ntp - 2 * j) % ntp)
        tok_share(j).wait_send()
    for j in range(chips):
        tok_copy(j).wait_send()
    for k in range(1, ntp):
        for l in range(local):
            down_copy(k, l).wait()
    each_send(lambda copy: copy.wait_send())
    passed = relayed(lambda *which: onward(*which).wait_send())
    for m, l in steps:
        passed(m, l)
        for d in range(1, nfs):
            forward(m, l, (f + d) % nfs).wait_send()


def move_weights(gate, up, down, tokens, nfs, ntp):
    local = EXPERTS // ntp
    width = gate.shape[2] * ntp // nfs
    rows, dcols = gate.shape[1], down.shape[2]
    dma = pltpu.SemaphoreType.DMA
    any_spec = pl.BlockSpec(memory_space=pl.ANY)
    bf = jnp.bfloat16
    ratio = nfs // ntp
    chips = ntp // 2
    passes = (2, local, chips - 1, 2, ratio)
    return pl.pallas_call(
        functools.partial(handoff, nfs, ntp),
        out_shape=(
            jax.ShapeDtypeStruct((local, rows * nfs, width), bf),
            jax.ShapeDtypeStruct((local, rows * nfs, width), bf),
            jax.ShapeDtypeStruct((local, down.shape[1], dcols * ntp), bf),
            jax.ShapeDtypeStruct((tokens.shape[0] * ntp, tokens.shape[1]), bf),
            jax.ShapeDtypeStruct((*passes, rows // 2, width), bf),
        ),
        in_specs=[any_spec] * 4,
        out_specs=(any_spec,) * 5,
        scratch_shapes=[
            [pltpu.VMEM(tokens.shape, bf), pltpu.VMEM(down.shape[1:], bf),
             pltpu.VMEM((rows, width), bf)],
            dma,
            dma((2, local, chips, 2, ratio, 2)),
            dma((2, local, nfs, 2)),
            dma((2, local, nfs)),
            dma(passes), dma(passes),
            dma((ntp - 1, local)), dma((ntp - 1, local)),
            dma((2, chips)), dma((ntp,)),
        ],
        compiler_params=pltpu.CompilerParams(collective_id=0, has_side_effects=True),
    )(gate, up, down, tokens)


def per_device(tokens, routes, route_weight, norm_gain, gate_train, up_train, down_train):
    nfs, ntp = lax.axis_size("fs"), lax.axis_size("tp")
    t = lax.axis_index("tp")
    bf = jnp.bfloat16
    gate_cast = (norm_gain[None, :, None] * gate_train).astype(bf)
    up_cast = (norm_gain[None, :, None] * up_train).astype(bf)
    down_cast = down_train.astype(bf)
    gate_serve, up_serve, down_serve, tok_all, _ = move_weights(
        gate_cast, up_cast, down_cast, tokens, nfs, ntp)
    local = EXPERTS // ntp
    n_tok = tokens.shape[0]
    routing = jnp.concatenate([routes.astype(jnp.float32), route_weight], axis=1)
    routing = lax.all_gather(routing, "tp", axis=0)
    routes_all = routing[:, :, :2].astype(jnp.int32)
    weight_all = routing[:, :, 2:]
    expert_ids = jnp.arange(EXPERTS, dtype=jnp.int32)
    named = routes_all[None] == expert_ids[:, None, None, None]
    chosen = jnp.any(named, axis=3)
    weight_e = jnp.sum(jnp.where(named, weight_all[None], 0.0), axis=3)
    count = chosen.astype(jnp.int32)
    slot = jnp.cumsum(count, axis=2) - count
    slot_ids = jnp.arange(CAP, dtype=jnp.int32)
    select = (chosen[:, :, None, :] & (slot[:, :, None, :] == slot_ids[None, None, :, None])).astype(bf)
    mine = lax.dynamic_slice_in_dim(select, t * local, local, axis=0)
    weight_mine = lax.dynamic_slice_in_dim(weight_e, t * local, local, axis=0)
    gate_h = jnp.einsum("td,ldf->ltf", tok_all, gate_serve, preferred_element_type=jnp.float32)
    up_h = jnp.einsum("td,ldf->ltf", tok_all, up_serve, preferred_element_type=jnp.float32)
    hidden = jax.nn.silu(gate_h) * up_h * weight_mine.reshape(local, -1)[:, :, None]
    hidden = hidden.astype(bf).reshape(local, ntp, n_tok, -1)
    packed = jnp.einsum("lbst,lbtf->lbsf", mine, hidden, preferred_element_type=jnp.float32).astype(bf)
    packed = lax.all_gather(packed, "tp", axis=0, tiled=True)
    dense = jnp.einsum("ebst,ebsf->btef", select, packed, preferred_element_type=jnp.float32).astype(bf)
    partial = jnp.dot(
        dense.reshape(ntp * n_tok, -1), down_cast.reshape(-1, down_cast.shape[2]),
        preferred_element_type=jnp.float32).astype(bf)
    ratio = nfs // ntp
    partial = partial.reshape(ntp, n_tok, ratio, -1)
    partial = lax.all_to_all(partial, "tp", split_axis=0, concat_axis=0, tiled=True)
    partial = partial.transpose(0, 2, 1, 3).reshape(nfs, n_tok, -1)
    partial = lax.all_to_all(partial, "fs", split_axis=0, concat_axis=0, tiled=True)
    moe_out = jnp.sum(partial.astype(jnp.float32), axis=0).astype(bf)
    return (gate_serve, up_serve, down_serve, moe_out)


def solution(mesh):
    return jax.shard_map(
        per_device,
        mesh=mesh,
        in_specs=(
            P(("grp", "tp"), None),
            P(("grp", "tp"), None),
            P(("grp", "tp"), None),
            P("fs"),
            P(None, "fs", "tp"),
            P(None, "fs", "tp"),
            P(None, "fs", "tp"),
        ),
        out_specs=(
            P(("grp", "tp"), None, "fs"),
            P(("grp", "tp"), None, "fs"),
            P(("grp", "tp"), "fs", None),
            P(("grp", "tp"), "fs"),
        ),
        check_vma=False,
    )
```

time: 686 us -> 546 us (0.80)
  Pallas kernels: 410 us -> 276 us
    pallas_call x1, Pallas kernels: 410 us -> 276 us  [move_weights(): pl.pallas_call(functools.partial(handoff, nfs, ntp), out_shape=(jax.Shape...]
where the time goes in v2:
time: 546 us; the launch traced here: 545 us
  Pallas kernels  276 us (51%)
  waiting for transfers between devices  81.3 us (15%)
  matrix products  53.8 us (10%)
  local copies, waits for them, and re-layouts  49.7 us (9%)
  blocking collectives  35.2 us (6%)
  other arithmetic  30.7 us (6%)
  between operations  14.1 us (3%)
    pallas_call x1, Pallas kernels, move_weights(): pl.pallas_call(functools.partial(handoff, nfs, ntp), out_shape=(jax.Shape...  276 us
    all_to_all x1, waiting for transfers between devices, per_device(): lax.all_to_all(partial, 'fs', split_axis=0, concat_axis=0, tiled=True)  47.8 us
    unnamed x10, local copies, waits for them, and re-layouts  34.9 us
    all_gather x1, waiting for transfers between devices, per_device(): packed = lax.all_gather(packed, 'tp', axis=0, tiled=True)  33.4 us
    all_to_all x1, blocking collectives, per_device(): lax.all_to_all(partial, 'tp', split_axis=0, concat_axis=0, tiled=True)  29 us
    convert_element_type x1, other arithmetic, per_device(): up_cast = (norm_gain[None, :, None] * up_train).astype(bf)  17 us
    dot_general x1, matrix products, per_device(): jnp.einsum('td,ldf->ltf', tok_all, gate_serve, preferred_element_type=jnp...  15.2 us
    dot_general x1, matrix products, per_device(): jnp.einsum('td,ldf->ltf', tok_all, up_serve, preferred_element_type=jnp.f...  15.1 us
  transfers between devices with their start and end apart: 2, of which 2 were waited for; matrix products, arithmetic and copies ran while one was open for 0% of the time, Pallas kernels for 0%

profile of v2, /device:TPU:0, one launch (start us, length us, event | category | flops | bytes accessed | tf_op | source)
XLA Modules:
  0.0 545.1 jit_solution(11479871407090429899)
XLA Ops:
  7.2 0.0 all-gather.3.cloned.1.call-start
  7.2 9.1 %convert_element_type.48.down = bf16[8,512,1024]{2,1,0:T(8,128)(2,1)} convert(f32[8,512,1024]{2,1,0:T(8,128)} %param.13) | non-fusion elementwise | flops 4194304 | bytes 25165824 | tf_op jit(solution)/shard_map/convert_element_type | solution.py:280
  16.4 6.2 %all-gather = f32[1024,4]{0,1:T(4,128)S(1)} all-gather(f32[256,4]{0,1:T(4,128)S(1)} %pad_maximum_fusion), channel_id=2, replica_groups=mesh['grp'=2,'fs'=4,'tp'=4] {'tp'}, dimensions={0}, use_global_device_ids=true | all-gather | bytes 20480 | tf_op jit(solution)/shard_map/all_gather | solution.py:286
  22.7 2.3 reduce-window.6
  24.9 0.3 slice_reduce_fusion
  25.2 0.1 convert_subtract_fusion
  25.3 0.9 fusion.9
  26.2 17.0 %multiply_convert_fusion = (bf16[8,1024,512]{2,1,0:T(8,128)(2,1)}, bf16[8,1024,512]{2,1,0:T(8,128)(2,1)}) fusion(f32[8,1024,512]{2,1,0:T(8,128)} %param.12, f32[1024]{0:T(1024)S(1)} %copy-done, f32[8,1024,512]{2,1,0:T(8,128)} %param.11), kind=kLoop, calls=%fused_computation | loop fusion | flops 16777216 | bytes 50335744 | tf_op jit(solution)/shard_map/convert_element_type | solution.py:279
  43.3 275.7 %shard_map.102 = (bf16[2,4096,512]{2,1,0:T(8,128)(2,1)}, bf16[2,4096,512]{2,1,0:T(8,128)(2,1)}, bf16[2,512,4096]{2,1,0:T(8,128)(2,1)}, bf16[1024,4096]{1,0:T(8,128)(2,1)}, bf16[2,2,1,2,1,512,512]{6,5,4,3,2,1,0:T(8,128)(2,1)}) custom-call(bf16[8,1024,512]{2,1,0:T(8,128)(2,1)} %get-tuple-element.15.gate, bf16[8,1024,512]{2,1,0:T(8,128)(2,1)} %get-tuple-element.14.up, ...), custom_call_target="tpu_custom_call" | custom-call | tf_op jit(solution)/shard_map/pallas_call | solution.py:248
  318.9 15.1 %fusion = f32[2,512,1024]{2,1,0:T(8,128)} fusion(bf16[2,4096,512]{2,1,0:T(8,128)(2,1)} %get-tuple-element.21, bf16[1024,4096]{1,0:T(8,128)(2,1)} %get-tuple-element.11), kind=kOutput, calls=%fused_computation.2 | convolution fusion | flops 8589934592 | bytes 20971520 | tf_op jit(solution)/shard_map/td,ldf->ltf/dot_general | solution.py:300
  334.0 15.2 %fusion.5 = bf16[2,1024,512]{1,2,0:T(8,128)(2,1)S(1)} fusion(f32[2,512,1024]{2,1,0:T(8,128)} %fusion, bf16[2,4096,512]{2,1,0:T(8,128)(2,1)} %get-tuple-element.20, bf16[1024,4096]{1,0:T(8,128)(2,1)} %get-tuple-element.11, f32[2,1024]{1,0:T(2,128)S(1)} %bitcast.68), kind=kOutput, calls=%fused_computation.9 | convolution fusion | flops 8597274624 | bytes 23076864 | tf_op jit(solution)/shard_map/td,ldf->ltf/dot_general | solution.py:299
  349.3 1.8 fusion.15
  351.1 33.4 %all-gather.3.cloned.1.call-done = bf16[8,4,128,512]{3,2,0,1:T(8,128)(2,1)} async-done(((bf16[2,4,128,512]{3,2,0,1:T(8,128)(2,1)}), bf16[8,4,128,512]{3,2,0,1:T(8,128)(2,1)}) %all-gather.3.cloned.1.call-update) | async-done | bytes 4194320 | tf_op jit(solution)/shard_map/all_gather | solution.py:304
  384.5 8.0 %convert_bitcast_fusion = bf16[4,256,8,512]{1,3,2,0:T(8,128)(2,1)} fusion(bf16[8,4,128,512]{3,2,0,1:T(8,128)(2,1)} %all-gather.3.cloned.1.call-done, s32[8,4,256]{2,0,1:T(8,128)S(1)} %convert_subtract_fusion, pred[8,4,256]{2,0,1:T(8,128)(4,1)S(1)} %fusion.19), kind=kOutput, calls=%fused_computation.6 | convolution fusion | flops 1080033280 | bytes 12623872 | tf_op jit(solution)/shard_map/ebst,ebsf->btef/dot_general | solution.py:305
  392.5 14.5 %copy.40 = bf16[4,256,8,512]{3,2,1,0:T(8,128)(2,1)} copy(bf16[4,256,8,512]{1,3,2,0:T(8,128)(2,1)} %convert_bitcast_fusion) | data formatting | bytes 16777216 | tf_op jit(solution)/shard_map/convert_element_type | solution.py:305
  407.1 12.4 %copy.48 = bf16[128,8,8,512]{3,1,2,0:T(8,128)(2,1)} copy(bf16[128,8,8,512]{3,2,1,0:T(8,128)(2,1)} %bitcast.62) | data formatting | bytes 16777216
  419.4 13.7 %convolution_convert_fusion = bf16[1024,1024]{1,0:T(8,128)(2,1)S(1)} fusion(bf16[1024,4096]{1,0:T(8,128)(2,1)} %bitcast.63, bf16[4096,1024]{1,0:T(8,128)(2,1)} %bitcast.61), kind=kOutput, calls=%fused_computation.20 | convolution fusion | flops 8590983168 | bytes 18874368 | tf_op jit(solution)/shard_map/dot_general | solution.py:306
  433.1 29.0 %all_to_all.10 = bf16[4,256,1,1024]{3,1,2,0:T(8,128)(2,1)} all-to-all(bf16[4,256,1,1024]{3,1,2,0:T(8,128)(2,1)S(1)} %bitcast.66), channel_id=1, replica_groups=mesh['grp'=2,'fs'=4,'tp'=4] {'tp'}, dimensions={0} | all-to-all | bytes 4194304 | tf_op jit(solution)/shard_map/all_to_all | solution.py:311
  462.0 4.6 all-to-all-start.1
  466.6 47.8 %all-to-all-done.1 = bf16[4,256,1024]{2,1,0:T(8,128)(2,1)S(1)} async-done(((bf16[4,256,1024]{2,1,0:T(8,128)(2,1)}), bf16[4,256,1024]{2,1,0:T(8,128)(2,1)S(1)}, u32[]{:S(2)}, u32[]{:S(2)}) %all-to-all-start.1) | async-done | bytes 2097184 | tf_op jit(solution)/shard_map/all_to_all | solution.py:313
  514.5 1.3 reduce_sum.22
  515.8 7.3 %copy.62 = bf16[2,4096,512]{2,1,0:T(8,128)(2,1)} copy(bf16[2,4096,512]{2,1,0:T(8,128)(2,1)} %get-tuple-element.20) | data formatting | bytes 16777216
  523.1 7.3 %copy.63 = bf16[2,4096,512]{2,1,0:T(8,128)(2,1)} copy(bf16[2,4096,512]{2,1,0:T(8,128)(2,1)} %get-tuple-element.21) | data formatting | bytes 16777216
  530.4 7.9 %copy.64 = bf16[2,512,4096]{2,1,0:T(8,128)(2,1)} copy(bf16[2,512,4096]{2,1,0:T(8,128)(2,1)} %get-tuple-element.22) | data formatting | bytes 16777216
  (16 shorter events, 0.1 us)
Async XLA Ops:
  7.2 377.4 %all-gather.3.cloned.1.call-start = ((), (), s32[]{:S(2)}) async-start(), calls=%async_computation.2 | async-start | bytes 5242880 | tf_op jit(solution)/shard_map/all_gather | solution.py:304
  7.2 9.1 %copy-start.1 = (s32[256,2]{0,1:T(2,128)S(1)}, s32[256,2]{0,1:T(2,128)}, u32[]{:S(2)}) copy-start(s32[256,2]{0,1:T(2,128)} %param.8) | copy-start | bytes 6148
  7.2 9.1 %copy-start.2 = (f32[256,2]{0,1:T(2,128)S(1)}, f32[256,2]{0,1:T(2,128)}, u32[]{:S(2)}) copy-start(f32[256,2]{0,1:T(2,128)} %param.9) | copy-start | bytes 6148
  7.2 19.0 %copy-start = (f32[1024]{0:T(1024)S(1)}, f32[1024]{0:T(1024)}, u32[]{:S(2)}) copy-start(f32[1024]{0:T(1024)} %param.10) | copy-start | bytes 12292
  462.0 52.4 %all-to-all-start.1 = ((bf16[4,256,1024]{2,1,0:T(8,128)(2,1)}), bf16[4,256,1024]{2,1,0:T(8,128)(2,1)S(1)}, u32[]{:S(2)}, u32[]{:S(2)}) async-start(bf16[4,256,1024]{2,1,0:T(8,128)(2,1)} %bitcast.64), calls=%async_computation.1 | async-start | bytes 4194304 | tf_op jit(solution)/shard_map/all_to_all | solution.py:313
Sparse Core Ops, SparseCore 0:
  351.2 33.2 all-gather.2
